TPU v7x, 32 devices: a whole 2x2x4 slice. The times are simulated.
32 devices in a mesh: grp: 2 (over y), sp: 4 (over z), tp: 4 (over x, core).
Axes of the slice: x: 2, y: 2, z: 4, core: 2. Of those that a mesh axis runs over, the one named last changes fastest.
Arguments:
- resid: bfloat16 [5120, 2048], P(('grp', 'sp'), 'tp'), parts along dimension 0, may hold values from -6 to 6
- queries: bfloat16 [5120, 2048], P(('grp', 'sp'), 'tp'), parts along dimension 0, may hold values from -150 to 150
- keys_values: bfloat16 [5120, 8, 128], P(('grp', 'sp'), 'tp'), parts along dimension 0, may hold values from -4.5 to 4.5
- sink: float32 [32], P('tp'), may hold values from 3 to 7
- out_weight: bfloat16 [2048, 2048], P('tp'), may hold values from -2.390625 to 2.390625
- norm_gain: float32 [2048], replicated, may hold values from 0.1 to 1.9
- gate_weight: bfloat16 [2048, 5632], P('sp', 'tp'), may hold values from -0.125 to 0.125
- up_weight: bfloat16 [2048, 5632], P('sp', 'tp'), may hold values from -0.125 to 0.125
- down_weight: bfloat16 [5632, 2048], P('tp', 'sp'), may hold values from -0.078125 to 0.078125
Outputs:
- mixed: bfloat16 [5120, 2048], P(('grp', 'sp'), 'tp'), parts along dimension 0
There are 2 independent parts, one for each index of `grp`. A program takes and returns all parts, laid end to end along the dimension named above; an argument that names none is the same for every part. Nothing has to cross between parts.
All inputs are finite; a program needn't handle non-finite values.
Results may differ from a plain program's by a relative error of at most 0.008.
Values may be sent and summed in bfloat16 or wider, within the bound.
A program may use at most 128 MiB of HBM per device.

v0:
```python
import jax
import jax.numpy as jnp
from jax import lax
from jax.sharding import PartitionSpec as P

HEAD_DIM = 64
WINDOW = 128
GRID_W = 64


def with_halo(cells, sides, width):
    for axis, dim in sides:
        count = lax.axis_size(axis)
        ends = count - 1
        head = lax.slice_in_dim(cells, 0, width, axis=dim)
        tail = lax.slice_in_dim(cells, cells.shape[dim] - width, cells.shape[dim], axis=dim)
        cells = jnp.concatenate(
            [
                lax.ppermute(tail, axis, [(i, (i + 1) % count) for i in range(ends)]),
                cells,
                lax.ppermute(head, axis, [((i + 1) % count, i) for i in range(ends)]),
            ],
            axis=dim,
        )
    return cells


def rotate(values, positions):
    quarter = 16
    inverse = 10000.0 ** (-jnp.arange(quarter, dtype=jnp.float32) / quarter)

    def turn(part, place):
        angle = place.astype(jnp.float32)[:, None] * inverse[None, :]
        cosine = jnp.cos(angle)[:, None, :]
        sine = jnp.sin(angle)[:, None, :]
        first, second = (part[..., :quarter], part[..., quarter:])
        return jnp.concatenate(
            [first * cosine - second * sine, second * cosine + first * sine], axis=-1
        )

    grid_row = positions // GRID_W
    grid_col = positions % GRID_W
    return jnp.concatenate(
        [turn(values[..., :32], grid_row), turn(values[..., 32:], grid_col)], axis=-1
    )


def body(
    resid, queries, keys_values, sink, out_weight, norm_gain, gate_weight, up_weight, down_weight
):
    tok = queries.shape[0]
    heads_here = queries.shape[1] // HEAD_DIM
    kv_here = keys_values.shape[1]
    group = heads_here // kv_here
    cols = resid.shape[1]
    offset = lax.axis_index("sp") * tok
    total_tokens = tok * lax.axis_size("sp")
    positions = offset + jnp.arange(tok, dtype=jnp.int32)
    rotated_q = rotate(
        queries.astype(jnp.float32).reshape(tok, heads_here, HEAD_DIM), positions
    ).astype(jnp.bfloat16)
    rotated_k = rotate(keys_values[..., :HEAD_DIM].astype(jnp.float32), positions).astype(
        jnp.bfloat16
    )
    joined = jnp.concatenate([rotated_k, keys_values[..., HEAD_DIM:]], axis=-1)
    padded = with_halo(joined, (("sp", 0),), WINDOW)
    blocks = tok // WINDOW
    key_blocks = jnp.stack(
        [padded[index * WINDOW : index * WINDOW + 3 * WINDOW] for index in range(blocks)]
    )
    grouped = rotated_q.reshape(blocks, WINDOW, kv_here, group, HEAD_DIM)
    scores = jnp.einsum(
        "nqkgd,njkd->nkgqj", grouped, key_blocks[..., :HEAD_DIM], preferred_element_type=jnp.float32
    ) * HEAD_DIM ** (-0.5)
    block_start = offset + WINDOW * jnp.arange(blocks, dtype=jnp.int32)
    query_pos = block_start[:, None] + jnp.arange(WINDOW, dtype=jnp.int32)[None, :]
    key_pos = block_start[:, None] - WINDOW + jnp.arange(3 * WINDOW, dtype=jnp.int32)[None, :]
    valid = (
        (jnp.abs(query_pos[:, :, None] - key_pos[:, None, :]) <= WINDOW)
        & (key_pos[:, None, :] >= 0)
        & (key_pos[:, None, :] < total_tokens)
    )
    scores = jnp.where(valid[:, None, None], scores, jnp.float32(-1e30))
    sink_grid = sink.reshape(kv_here, group)[None, :, :, None]
    top = jnp.maximum(jnp.max(scores, axis=-1), sink_grid)
    expo = jnp.exp(scores - top[..., None])
    denom = jnp.sum(expo, axis=-1) + jnp.exp(sink_grid - top)
    probs = (expo / denom[..., None]).astype(jnp.bfloat16)
    attended = jnp.einsum(
        "nkgqj,njkd->nqkgd", probs, key_blocks[..., HEAD_DIM:], preferred_element_type=jnp.float32
    )
    attended = attended.astype(jnp.bfloat16).reshape(tok, heads_here * HEAD_DIM)
    attn_rows, resid_rows = (
        lax.all_to_all(attended, "tp", split_axis=0, concat_axis=1, tiled=True),
        lax.all_to_all(resid, "tp", split_axis=0, concat_axis=1, tiled=True),
    )
    whole_out = lax.all_gather(out_weight, "tp", axis=0, tiled=True)
    stream_part = (
        resid_rows.astype(jnp.float32)
        + jnp.dot(attn_rows, whole_out, preferred_element_type=jnp.float32)
    ).astype(jnp.bfloat16)
    stream = lax.all_gather(stream_part, "tp", axis=0, tiled=True)
    stream_cols = lax.dynamic_slice_in_dim(stream, lax.axis_index("tp") * cols, cols, 1)
    widened = stream.astype(jnp.float32)
    normed = (
        widened * lax.rsqrt(jnp.mean(widened * widened, axis=-1, keepdims=True) + 1e-06) * norm_gain
    ).astype(jnp.bfloat16)
    gate = jnp.dot(
        normed,
        lax.all_gather(gate_weight, "sp", axis=0, tiled=True),
        preferred_element_type=jnp.float32,
    )
    up = jnp.dot(
        normed,
        lax.all_gather(up_weight, "sp", axis=0, tiled=True),
        preferred_element_type=jnp.float32,
    )
    hidden = (jax.nn.silu(gate) * up).astype(jnp.bfloat16)
    terms = jnp.dot(
        hidden,
        lax.all_gather(down_weight, "sp", axis=1, tiled=True),
        preferred_element_type=jnp.float32,
    )
    summed = lax.psum_scatter(
        terms.astype(jnp.bfloat16), "tp", scatter_dimension=1, tiled=True
    ).astype(jnp.float32)
    return (stream_cols.astype(jnp.float32) + summed).astype(jnp.bfloat16)


def solution(mesh):
    return jax.shard_map(
        body,
        mesh=mesh,
        in_specs=(
            P(("grp", "sp"), "tp"),
            P(("grp", "sp"), "tp"),
            P(("grp", "sp"), "tp", None),
            P("tp"),
            P("tp", None),
            P(),
            P("sp", "tp"),
            P("sp", "tp"),
            P("tp", "sp"),
        ),
        out_specs=P(("grp", "sp"), "tp"),
        check_vma=False,
    )
```

profile of v0, /device:TPU:0, one launch (start us, length us, event | category | flops | bytes accessed | tf_op | source)
XLA Modules:
  0.0 493.6 jit_solution(14125125992527969314)
XLA Ops:
  6.5 0.7 all-gather.6.cloned.1.call-update
  7.3 1.7 fusion.49
  8.9 0.2 copy.43
  9.2 0.2 copy.44
  9.4 0.4 multiply_cosine_fusion.1
  9.9 5.0 %collective-permute-start = (bf16[128,2,128]{0,2,1:T(8,128)(2,1)S(1)}, bf16[128,2,128]{0,2,1:T(8,128)(2,1)S(1)}, u32[]{:S(2)}, u32[]{:S(2)}) collective-permute-start(bf16[128,2,128]{0,2,1:T(8,128)(2,1)S(1)} %get-tuple-element.12), channel_id=1, source_target_pairs={{0,4},{4,8},{8,12},{1,5},{5,9},{9,13},{2,6},{6,10},{10,14},{3,7},{... | collective-permute-start | bytes 196616 | tf_op jit(solution)/shard_map/ppermute | solution.py:19
  14.9 1.3 collective-permute-start.1
  16.2 3.5 all-to-all-start
  19.7 0.3 copy.32
  20.1 0.1 convert.39
  20.2 0.1 iota_add_fusion.1
  20.2 0.1 fusion.36
  20.3 0.1 iota_add_fusion
  20.4 0.2 subtract_convert_fusion.1
  20.6 1.2 fusion.11
  21.8 0.2 concatenate.29
  22.0 0.2 concatenate.30
  22.2 0.2 concatenate.31
  22.5 0.2 concatenate.32
  22.7 0.1 max.17
  23.0 1.3 fusion.1
  24.3 0.1 broadcast_maximum_fusion
  24.4 1.9 fusion
  26.3 0.1 exponential_add_fusion
  26.4 2.3 fusion.9
  28.7 1.6 copy.38
  30.3 1.6 all_to_all.26
  31.9 5.0 %all-to-all-done = bf16[4,160,512]{2,1,0:T(8,128)(2,1)S(1)} async-done(((bf16[4,160,512]{2,1,0:T(8,128)(2,1)}), bf16[4,160,512]{2,1,0:T(8,128)(2,1)S(1)}, u32[]{:S(2)}, u32[]{:S(2)}) %all-to-all-start) | async-done | bytes 655392 | tf_op jit(solution)/shard_map/all_to_all | solution.py:95
  36.9 3.5 all-to-all-start.1
  40.5 0.2 convert_bitcast_fusion
  40.6 0.1 copy.45
  40.8 17.3 %all-to-all-done.1 = bf16[4,160,512]{2,1,0:T(8,128)(2,1)S(1)} async-done(((bf16[4,160,512]{2,1,0:T(8,128)(2,1)}), bf16[4,160,512]{2,1,0:T(8,128)(2,1)S(1)}, u32[]{:S(2)}, u32[]{:S(2)}) %all-to-all-start.1) | async-done | bytes 655392 | tf_op jit(solution)/shard_map/all_to_all | solution.py:94
  58.0 0.1 copy.46
  58.1 25.6 %all-gather.6.cloned.1.call-done = bf16[2048,2048]{1,0:T(8,128)(2,1)} async-done(((bf16[512,2048]{1,0:T(8,128)(2,1)}), bf16[2048,2048]{1,0:T(8,128)(2,1)}) %all-gather.6.cloned.1.call-update) | async-done | bytes 8388624 | tf_op jit(solution)/shard_map/all_gather | solution.py:97
  83.7 5.7 %fusion.7 = bf16[160,2048]{1,0:T(8,128)(2,1)} fusion(f32[160,2048]{1,0:T(8,128)S(1)} %bitcast.70, bf16[160,2048]{1,0:T(8,128)(2,1)S(1)} %bitcast.71, bf16[2048,2048]{1,0:T(8,128)(2,1)} %all-gather.6.cloned.1.call-done), kind=kOutput, calls=%fused_computation.15 | convolution fusion | flops 1342832640 | bytes 11010048 | tf_op jit(solution)/shard_map/dot_general | solution.py:100
  89.5 0.7 all-gather.10.cloned.1.call-update
  90.2 0.5 all-gather.12.cloned.1.call-update
  90.8 0.5 all-gather.14.cloned.1.call-update
  91.3 0.2 reduce-scatter.2.cloned.1.call-start
  91.6 23.8 %all-gather.8.cloned.1.call-done = bf16[640,2048]{1,0:T(8,128)(2,1)} async-done(((bf16[160,2048]{1,0:T(8,128)(2,1)}), bf16[640,2048]{1,0:T(8,128)(2,1)}) %all-gather.8.cloned.1.call-update) | async-done | bytes 2621456 | tf_op jit(solution)/shard_map/all_gather | solution.py:102
  115.4 2.3 fusion.2
  117.8 106.0 %all-gather.10.cloned.1.call-done = bf16[2048,1408]{1,0:T(8,128)(2,1)} async-done(((bf16[512,1408]{1,0:T(8,128)(2,1)}), bf16[2048,1408]{1,0:T(8,128)(2,1)}) %all-gather.10.cloned.1.call-update) | async-done | bytes 5767184 | tf_op jit(solution)/shard_map/all_gather | solution.py:110
  223.7 9.5 %fusion.14 = f32[640,1408]{1,0:T(8,128)} fusion(bf16[2048,1408]{1,0:T(8,128)(2,1)} %all-gather.10.cloned.1.call-done, bf16[640,2048]{1,0:T(8,128)(2,1)} %all-gather.8.cloned.1.call-done, f32[2048]{0:T(1024)S(1)} %copy-done.2, f32[640]{0:T(1024)S(1)} %add_rsqrt_fusion), kind=kOutput, calls=%fused_computation.23 | convolution fusion | flops 3696230400 | bytes 12003840 | tf_op jit(solution)/shard_map/dot_general | solution.py:108
  233.2 96.9 %all-gather.12.cloned.1.call-done = bf16[2048,1408]{1,0:T(8,128)(2,1)} async-done(((bf16[512,1408]{1,0:T(8,128)(2,1)}), bf16[2048,1408]{1,0:T(8,128)(2,1)}) %all-gather.12.cloned.1.call-update) | async-done | bytes 5767184 | tf_op jit(solution)/shard_map/all_gather | solution.py:115
  330.1 106.4 %all-gather.14.cloned.1.call-done = bf16[1408,2048]{1,0:T(8,128)(2,1)} async-done(((bf16[1408,512]{1,0:T(8,128)(2,1)}), bf16[1408,2048]{1,0:T(8,128)(2,1)}) %all-gather.14.cloned.1.call-update) | async-done | bytes 5767184 | tf_op jit(solution)/shard_map/all_gather | solution.py:121
  436.5 15.3 %convolution_convert_fusion = bf16[640,2048]{1,0:T(8,128)(2,1)} fusion(bf16[1408,2048]{1,0:T(8,128)(2,1)} %all-gather.14.cloned.1.call-done, bf16[2048,1408]{1,0:T(8,128)(2,1)} %all-gather.12.cloned.1.call-done, f32[640,1408]{1,0:T(8,128)} %fusion.14, bf16[640,2048]{1,0:T(8,128)(2,1)S(1)} %copy-done, f32[2048]{0:T(1024)S(1)} %copy-done.2, ...), kind=kOutput, calls=%fused_computation.13 | convolution fusion | flops 7393935360 | bytes 20392448 | tf_op jit(solution)/shard_map/dot_general | solution.py:119
  451.9 32.8 %reduce-scatter.2.cloned.1.call-done = bf16[640,512]{1,0:T(8,128)(2,1)} async-done(((bf16[640,2048]{1,0:T(8,128)(2,1)}), bf16[640,512]{1,0:T(8,128)(2,1)}) %reduce-scatter.2.cloned.1.call-update) | async-done | bytes 655376 | tf_op jit(solution)/shard_map/reduce_scatter | solution.py:124
  484.7 2.1 add_convert_fusion
  (37 shorter events, 0.7 us)
Async XLA Ops:
  6.5 13.2 %copy-start.1 = (bf16[640,512]{1,0:T(8,128)(2,1)S(1)}, bf16[640,512]{1,0:T(8,128)(2,1)}, u32[]{:S(2)}) copy-start(bf16[640,512]{1,0:T(8,128)(2,1)} %param.10) | copy-start | bytes 1966084
  6.5 77.1 %all-gather.6.cloned.1.call-start = ((), (), s32[]{:S(2)}) async-start(), calls=%async_computation.3 | async-start | bytes 10485760 | tf_op jit(solution)/shard_map/all_gather | solution.py:97
  9.9 12.9 %collective-permute-start = (bf16[128,2,128]{0,2,1:T(8,128)(2,1)S(1)}, bf16[128,2,128]{0,2,1:T(8,128)(2,1)S(1)}, u32[]{:S(2)}, u32[]{:S(2)}) collective-permute-start(bf16[128,2,128]{0,2,1:T(8,128)(2,1)S(1)} %get-tuple-element.12), channel_id=1, source_target_pairs={{0,4},{4,8},{8,12},{1,5},{5,9},{9,13},{2,6},{6,10},{10,14},{3,7},{... | collective-permute-start | bytes 196616 | tf_op jit(solution)/shard_map/ppermute | solution.py:19
  14.9 8.1 %collective-permute-start.1 = (bf16[128,2,128]{0,2,1:T(8,128)(2,1)S(1)}, bf16[128,2,128]{0,2,1:T(8,128)(2,1)S(1)}, u32[]{:S(2)}, u32[]{:S(2)}) collective-permute-start(bf16[128,2,128]{0,2,1:T(8,128)(2,1)S(1)} %get-tuple-element.11), channel_id=1, source_target_pairs={{4,0},{8,4},{12,8},{5,1},{9,5},{13,9},{6,2},{10,6},{14,10},{7,3},{... | collective-permute-start | bytes 196616 | tf_op jit(solution)/shard_map/ppermute | solution.py:21
  16.2 20.7 %all-to-all-start = ((bf16[4,160,512]{2,1,0:T(8,128)(2,1)}), bf16[4,160,512]{2,1,0:T(8,128)(2,1)S(1)}, u32[]{:S(2)}, u32[]{:S(2)}) async-start(bf16[4,160,512]{2,1,0:T(8,128)(2,1)} %bitcast), calls=%async_computation | async-start | bytes 1310720 | tf_op jit(solution)/shard_map/all_to_all | solution.py:95
  20.0 2.7 copy-start.3
  36.9 21.1 %all-to-all-start.1 = ((bf16[4,160,512]{2,1,0:T(8,128)(2,1)}), bf16[4,160,512]{2,1,0:T(8,128)(2,1)S(1)}, u32[]{:S(2)}, u32[]{:S(2)}) async-start(bf16[4,160,512]{2,1,0:T(8,128)(2,1)} %all_to_all.26), calls=%async_computation.1 | async-start | bytes 1310720 | tf_op jit(solution)/shard_map/all_to_all | solution.py:94
  40.4 75.0 %all-gather.8.cloned.1.call-start = ((), (), s32[]{:S(2)}) async-start(), calls=%async_computation.4 | async-start | bytes 3276800 | tf_op jit(solution)/shard_map/all_gather | solution.py:102
  89.4 134.3 %copy-start.2 = (f32[2048]{0:T(1024)S(1)}, f32[2048]{0:T(1024)}, u32[]{:S(2)}) copy-start(f32[2048]{0:T(1024)} %param.14) | copy-start | bytes 24580
  89.4 134.3 %all-gather.10.cloned.1.call-start = ((), (), s32[]{:S(2)}) async-start(), calls=%async_computation.5 | async-start | bytes 7208960 | tf_op jit(solution)/shard_map/all_gather | solution.py:110
  90.2 239.9 %all-gather.12.cloned.1.call-start = ((), (), s32[]{:S(2)}) async-start(), calls=%async_computation.6 | async-start | bytes 7208960 | tf_op jit(solution)/shard_map/all_gather | solution.py:115
  90.8 345.8 %all-gather.14.cloned.1.call-start = ((), (), s32[]{:S(2)}) async-start(), calls=%async_computation.7 | async-start | bytes 7208960 | tf_op jit(solution)/shard_map/all_gather | solution.py:121
  91.3 393.3 %reduce-scatter.2.cloned.1.call-start = ((), (), s32[]{:S(2)}) async-start(), calls=%async_computation.8 | async-start | bytes 3276800 | tf_op jit(solution)/shard_map/reduce_scatter | solution.py:124
  117.7 318.8 %copy-start = (bf16[640,2048]{1,0:T(8,128)(2,1)S(1)}, bf16[640,2048]{1,0:T(8,128)(2,1)}, u32[]{:S(2)}) copy-start(bf16[640,2048]{1,0:T(8,128)(2,1)} %all-gather.8.cloned.1.call-done) | copy-start | bytes 7864324
Sparse Core Ops, SparseCore 0:
  8.9 74.7 all-gather.5
  89.6 25.8 all-gather.7
  117.0 106.6 all-gather.9
  225.1 104.9 all-gather.11
  331.5 104.9 all-gather.13
  452.0 32.6 reduce-scatter.1
where the time goes:
time: 494 us
  waiting for transfers between devices  416 us (84%)
  matrix products  34.2 us (7%)
  between operations  13.8 us (3%)
  starting transfers between devices  13.6 us (3%)
  other arithmetic  8.95 us (2%)
  local copies, waits for them, and re-layouts  6.91 us (1%)
    all_gather x1, waiting for transfers between devices, body(): lax.all_gather(down_weight, 'sp', axis=1, tiled=True)  106 us
    all_gather x1, waiting for transfers between devices, body(): lax.all_gather(gate_weight, 'sp', axis=0, tiled=True)  106 us
    all_gather x1, waiting for transfers between devices, body(): lax.all_gather(up_weight, 'sp', axis=0, tiled=True)  96.9 us
    reduce_scatter x1, waiting for transfers between devices, body(): lax.psum_scatter(terms.astype(jnp.bfloat16), 'tp', scatter_dimension=1, t...  32.8 us
    all_gather x1, waiting for transfers between devices, body(): whole_out = lax.all_gather(out_weight, 'tp', axis=0, tiled=True)  25.6 us
    all_gather x1, waiting for transfers between devices, body(): stream = lax.all_gather(stream_part, 'tp', axis=0, tiled=True)  23.8 us
    all_to_all x1, waiting for transfers between devices, body(): lax.all_to_all(attended, 'tp', split_axis=0, concat_axis=1, tiled=True)  17.3 us
    dot_general x1, matrix products, body(): jnp.dot(hidden, lax.all_gather(down_weight, 'sp', axis=1, tiled=True), pr...  15.3 us
  transfers between devices with their start and end apart: 10, of which 8 were waited for; matrix products, arithmetic and copies ran while one was open for 5% of the time, Pallas kernels for 0%

commit v1 on v0

--- a/solution.py
+++ b/solution.py
@@ -43,6 +43,13 @@
     return jnp.concatenate(
         [turn(values[..., :32], grid_row), turn(values[..., 32:], grid_col)], axis=-1
     )
+
+
+def share(weight, axis):
+    parts = lax.axis_size("grp")
+    size = weight.shape[axis] // parts
+    part = lax.dynamic_slice_in_dim(weight, lax.axis_index("grp") * size, size, axis)
+    return lax.all_gather(part, ("sp", "grp"), axis=axis, tiled=True)
 
 
 def body(
@@ -107,18 +114,18 @@
     ).astype(jnp.bfloat16)
     gate = jnp.dot(
         normed,
-        lax.all_gather(gate_weight, "sp", axis=0, tiled=True),
+        share(gate_weight, 0),
         preferred_element_type=jnp.float32,
     )
     up = jnp.dot(
         normed,
-        lax.all_gather(up_weight, "sp", axis=0, tiled=True),
+        share(up_weight, 0),
         preferred_element_type=jnp.float32,
     )
     hidden = (jax.nn.silu(gate) * up).astype(jnp.bfloat16)
     terms = jnp.dot(
         hidden,
-        lax.all_gather(down_weight, "sp", axis=1, tiled=True),
+        share(down_weight, 1),
         preferred_element_type=jnp.float32,
     )
     summed = lax.psum_scatter(

time: 494 us -> 454 us (0.919)
  waiting for transfers between devices: 416 us -> 359 us
  local copies, waits for them, and re-layouts: 6.91 us -> 18.8 us
    all_gather x3, waiting for transfers between devices: 309 us -> 269 us  [share(): return lax.all_gather(part, ('sp', 'grp'), axis=axis, tiled=True)]
    all_gather x1, waiting for transfers between devices: 25.6 us -> 18.3 us  [body(): whole_out = lax.all_gather(out_weight, 'tp', axis=0, tiled=True)]
    all_to_all x1, waiting for transfers between devices: 4.96 us -> 0.01 us  [body(): lax.all_to_all(resid, 'tp', split_axis=0, concat_axis=1, tiled=True)]
  transfers between devices with their start and end apart: 10 -> 10, of which waited for: 8 -> 7; matrix products, arithmetic and copies ran while one was open for 5% -> 9% of each run, Pallas kernels for 0% -> 0%
where the time goes in v1:
time: 454 us
  waiting for transfers between devices  359 us (79%)
  matrix products  36.7 us (8%)
  local copies, waits for them, and re-layouts  18.8 us (4%)
  starting transfers between devices  15 us (3%)
  between operations  13.8 us (3%)
  other arithmetic  10.7 us (2%)
    all_gather x3, waiting for transfers between devices, share(): return lax.all_gather(part, ('sp', 'grp'), axis=axis, tiled=True)  269 us
    reduce_scatter x1, waiting for transfers between devices, body(): lax.psum_scatter(terms.astype(jnp.bfloat16), 'tp', scatter_dimension=1, t...  32.7 us
    all_gather x1, waiting for transfers between devices, body(): stream = lax.all_gather(stream_part, 'tp', axis=0, tiled=True)  21.3 us
    all_gather x1, waiting for transfers between devices, body(): whole_out = lax.all_gather(out_weight, 'tp', axis=0, tiled=True)  18.3 us
    all_to_all x1, waiting for transfers between devices, body(): lax.all_to_all(attended, 'tp', split_axis=0, concat_axis=1, tiled=True)  17.4 us
    dot_general x1, matrix products, body(): jnp.dot(hidden, share(down_weight, 1), preferred_element_type=jnp.float32)  16.1 us
    dot_general x1, matrix products, body(): jnp.dot(normed, share(gate_weight, 0), preferred_element_type=jnp.float32)  9.45 us
  transfers between devices with their start and end apart: 10, of which 7 were waited for; matrix products, arithmetic and copies ran while one was open for 9% of the time, Pallas kernels for 0%

profile of v1, /device:TPU:0, one launch (start us, length us, event | category | flops | bytes accessed | tf_op | source)
XLA Modules:
  0.0 453.8 jit_solution(18037443302899409441)
XLA Ops:
  6.5 0.7 all-gather.6.cloned.1.call-update
  7.3 1.7 fusion.49
  9.0 0.2 copy.43
  9.2 0.2 copy.44
  9.4 0.4 multiply_cosine_fusion.1
  9.9 0.7 fusion.48
  10.6 5.6 %collective-permute-start = (bf16[128,2,128]{0,2,1:T(8,128)(2,1)}, bf16[128,2,128]{0,2,1:T(8,128)(2,1)}, u32[]{:S(2)}, u32[]{:S(2)}) collective-permute-start(bf16[128,2,128]{0,2,1:T(8,128)(2,1)} %get-tuple-element.12), channel_id=1, source_target_pairs={{0,4},{4,8},{8,12},{1,5},{5,9},{9,13},{2,6},{6,10},{10,14},{3,7},{... | collective-permute-start | bytes 196616 | tf_op jit(solution)/shard_map/ppermute | solution.py:19
  16.2 1.3 collective-permute-start.1
  17.5 3.5 all-to-all-start
  21.0 1.4 copy.32
  22.5 0.1 convert.39
  22.8 0.9 subtract_convert_fusion.1
  23.7 1.2 fusion.11
  24.9 1.1 concatenate.29
  26.0 0.7 copy.33
  26.7 1.1 concatenate.30
  27.8 0.7 copy.34
  28.5 0.2 concatenate.31
  28.7 0.7 copy.35
  29.4 0.2 concatenate.32
  29.7 0.1 max.17
  29.8 0.9 fusion.30
  30.8 2.3 fusion.1
  33.2 1.9 fusion
  35.1 0.1 exponential_add_fusion
  35.2 3.1 fusion.9
  38.3 2.8 copy.38
  41.0 1.6 all_to_all.26
  42.6 4.2 all-to-all-start.1
  46.9 0.2 convert_bitcast_fusion
  47.0 0.1 copy.45
  47.2 17.4 %all-to-all-done.1 = bf16[4,160,512]{2,1,0:T(8,128)(2,1)} async-done(((bf16[4,160,512]{2,1,0:T(8,128)(2,1)}), bf16[4,160,512]{2,1,0:T(8,128)(2,1)}, u32[]{:S(2)}, u32[]{:S(2)}) %all-to-all-start.1) | async-done | bytes 655392 | tf_op jit(solution)/shard_map/all_to_all | solution.py:101
  64.5 1.2 copy.46
  65.7 18.3 %all-gather.6.cloned.1.call-done = bf16[2048,2048]{1,0:T(8,128)(2,1)} async-done(((bf16[512,2048]{1,0:T(8,128)(2,1)}), bf16[2048,2048]{1,0:T(8,128)(2,1)}) %all-gather.6.cloned.1.call-update) | async-done | bytes 8388624 | tf_op jit(solution)/shard_map/all_gather | solution.py:104
  84.0 5.8 %fusion.7 = bf16[160,2048]{1,0:T(8,128)(2,1)} fusion(f32[160,2048]{1,0:T(8,128)S(1)} %bitcast.70, bf16[160,2048]{1,0:T(8,128)(2,1)S(1)} %bitcast.71, bf16[2048,2048]{1,0:T(8,128)(2,1)} %all-gather.6.cloned.1.call-done), kind=kOutput, calls=%fused_computation.15 | convolution fusion | flops 1342832640 | bytes 11010048 | tf_op jit(solution)/shard_map/dot_general | solution.py:107
  89.8 0.9 constant_dynamic-slice_fusion.2
  90.8 2.0 constant_dynamic-slice_fusion.1
  92.9 1.0 constant_dynamic-slice_fusion
  93.9 0.2 reduce-scatter.2.cloned.1.call-start
  94.1 21.3 %all-gather.8.cloned.1.call-done = bf16[640,2048]{1,0:T(8,128)(2,1)} async-done(((bf16[160,2048]{1,0:T(8,128)(2,1)}), bf16[640,2048]{1,0:T(8,128)(2,1)}) %all-gather.8.cloned.1.call-update) | async-done | bytes 2621456 | tf_op jit(solution)/shard_map/all_gather | solution.py:109
  115.4 2.3 fusion.2
  117.8 92.2 %all-gather.10.cloned.1.call-done = bf16[2048,1408]{1,0:T(8,128)(2,1)} async-done(((bf16[256,1408]{1,0:T(8,128)(2,1)}), bf16[2048,1408]{1,0:T(8,128)(2,1)}) %all-gather.10.cloned.1.call-update) | async-done | bytes 5767184 | tf_op jit(solution)/shard_map/all_gather | solution.py:52
  210.0 9.5 %fusion.14 = f32[640,1408]{1,0:T(8,128)} fusion(bf16[2048,1408]{1,0:T(8,128)(2,1)} %all-gather.10.cloned.1.call-done, bf16[640,2048]{1,0:T(8,128)(2,1)} %all-gather.8.cloned.1.call-done, f32[2048]{0:T(1024)S(1)} %copy-done.4, f32[640]{0:T(1024)S(1)} %add_rsqrt_fusion), kind=kOutput, calls=%fused_computation.23 | convolution fusion | flops 3696230400 | bytes 12003840 | tf_op jit(solution)/shard_map/dot_general | solution.py:115
  219.4 83.1 %all-gather.12.cloned.1.call-done = bf16[2048,1408]{1,0:T(8,128)(2,1)} async-done(((bf16[256,1408]{1,0:T(8,128)(2,1)}), bf16[2048,1408]{1,0:T(8,128)(2,1)}) %all-gather.12.cloned.1.call-update) | async-done | bytes 5767184 | tf_op jit(solution)/shard_map/all_gather | solution.py:52
  302.5 93.2 %all-gather.14.cloned.1.call-done = bf16[1408,2048]{1,0:T(8,128)(2,1)} async-done(((bf16[1408,256]{1,0:T(8,128)(2,1)}), bf16[1408,2048]{1,0:T(8,128)(2,1)}) %all-gather.14.cloned.1.call-update) | async-done | bytes 5767184 | tf_op jit(solution)/shard_map/all_gather | solution.py:52
  395.8 16.1 %convolution_convert_fusion = bf16[640,2048]{1,0:T(8,128)(2,1)} fusion(bf16[1408,2048]{1,0:T(8,128)(2,1)} %all-gather.14.cloned.1.call-done, bf16[2048,1408]{1,0:T(8,128)(2,1)} %all-gather.12.cloned.1.call-done, f32[640,1408]{1,0:T(8,128)} %fusion.14, bf16[640,2048]{1,0:T(8,128)(2,1)} %all-gather.8.cloned.1.call-done, f32[2048]{0:T(1024)S(1)} %copy-done.4, ...), kind=kOutput, calls=%fused_computation.13 | convolution fusion | flops 7393935360 | bytes 20392448 | tf_op jit(solution)/shard_map/dot_general | solution.py:126
  411.9 32.7 %reduce-scatter.2.cloned.1.call-done = bf16[640,512]{1,0:T(8,128)(2,1)} async-done(((bf16[640,2048]{1,0:T(8,128)(2,1)}), bf16[640,512]{1,0:T(8,128)(2,1)}) %reduce-scatter.2.cloned.1.call-update) | async-done | bytes 655376 | tf_op jit(solution)/shard_map/reduce_scatter | solution.py:131
  444.7 2.3 add_convert_fusion
  (44 shorter events, 0.9 us)
Async XLA Ops:
  6.5 83.3 %copy-start = (bf16[512,1408]{1,0:T(8,128)(2,1)S(1)}, bf16[512,1408]{1,0:T(8,128)(2,1)}, u32[]{:S(2)}) copy-start(bf16[512,1408]{1,0:T(8,128)(2,1)} %param.15) | copy-start | bytes 4325380
  6.5 77.4 %all-gather.6.cloned.1.call-start = ((), (), s32[]{:S(2)}) async-start(), calls=%async_computation.3 | async-start | bytes 10485760 | tf_op jit(solution)/shard_map/all_gather | solution.py:104
  10.6 19.1 %collective-permute-start = (bf16[128,2,128]{0,2,1:T(8,128)(2,1)}, bf16[128,2,128]{0,2,1:T(8,128)(2,1)}, u32[]{:S(2)}, u32[]{:S(2)}) collective-permute-start(bf16[128,2,128]{0,2,1:T(8,128)(2,1)} %get-tuple-element.12), channel_id=1, source_target_pairs={{0,4},{4,8},{8,12},{1,5},{5,9},{9,13},{2,6},{6,10},{10,14},{3,7},{... | collective-permute-start | bytes 196616 | tf_op jit(solution)/shard_map/ppermute | solution.py:19
  16.2 14.6 %collective-permute-start.1 = (bf16[128,2,128]{0,2,1:T(8,128)(2,1)}, bf16[128,2,128]{0,2,1:T(8,128)(2,1)S(1)}, u32[]{:S(2)}, u32[]{:S(2)}) collective-permute-start(bf16[128,2,128]{0,2,1:T(8,128)(2,1)} %get-tuple-element.11), channel_id=1, source_target_pairs={{4,0},{8,4},{12,8},{5,1},{9,5},{13,9},{6,2},{10,6},{14,10},{7,3},{... | collective-permute-start | bytes 196616 | tf_op jit(solution)/shard_map/ppermute | solution.py:21
  17.5 25.1 %all-to-all-start = ((bf16[4,160,512]{2,1,0:T(8,128)(2,1)}), bf16[4,160,512]{2,1,0:T(8,128)(2,1)S(1)}, u32[]{:S(2)}, u32[]{:S(2)}) async-start(bf16[4,160,512]{2,1,0:T(8,128)(2,1)} %bitcast), calls=%async_computation | async-start | bytes 1310720 | tf_op jit(solution)/shard_map/all_to_all | solution.py:102
  22.5 7.2 %copy-start.5 = (f32[8]{0:T(128)S(1)}, f32[8]{0:T(128)}, u32[]{:S(2)}) copy-start(f32[8]{0:T(128)} %param.12) | copy-start | bytes 100
  28.7 2.1 copy-start.3
  42.6 21.9 %all-to-all-start.1 = ((bf16[4,160,512]{2,1,0:T(8,128)(2,1)}), bf16[4,160,512]{2,1,0:T(8,128)(2,1)}, u32[]{:S(2)}, u32[]{:S(2)}) async-start(bf16[4,160,512]{2,1,0:T(8,128)(2,1)} %all_to_all.26), calls=%async_computation.1 | async-start | bytes 1310720 | tf_op jit(solution)/shard_map/all_to_all | solution.py:101
  46.8 68.6 %all-gather.8.cloned.1.call-start = ((), (), s32[]{:S(2)}) async-start(), calls=%async_computation.4 | async-start | bytes 3276800 | tf_op jit(solution)/shard_map/all_gather | solution.py:109
  89.7 3.2 copy-start.2
  89.7 120.2 %all-gather.10.cloned.1.call-start = ((), (), s32[]{:S(2)}) async-start(), calls=%async_computation.5 | async-start | bytes 6488064 | tf_op jit(solution)/shard_map/all_gather | solution.py:52
  90.8 119.2 %copy-start.4 = (f32[2048]{0:T(1024)S(1)}, f32[2048]{0:T(1024)}, u32[]{:S(2)}) copy-start(f32[2048]{0:T(1024)} %param.14) | copy-start | bytes 24580
  90.8 211.8 %all-gather.12.cloned.1.call-start = ((), (), s32[]{:S(2)}) async-start(), calls=%async_computation.6 | async-start | bytes 6488064 | tf_op jit(solution)/shard_map/all_gather | solution.py:52
  92.9 302.9 %all-gather.14.cloned.1.call-start = ((), (), s32[]{:S(2)}) async-start(), calls=%async_computation.7 | async-start | bytes 6488064 | tf_op jit(solution)/shard_map/all_gather | solution.py:52
  93.9 350.7 %reduce-scatter.2.cloned.1.call-start = ((), (), s32[]{:S(2)}) async-start(), calls=%async_computation.8 | async-start | bytes 3276800 | tf_op jit(solution)/shard_map/reduce_scatter | solution.py:131
  395.8 51.2 %copy-start.1 = (bf16[512,1408]{1,0:T(8,128)(2,1)S(1)}, bf16[512,1408]{1,0:T(8,128)(2,1)}, u32[]{:S(2)}) copy-start(bf16[512,1408]{1,0:T(8,128)(2,1)} %param.15) | copy-start | bytes 4325380
Sparse Core Ops, SparseCore 0:
  8.9 75.0 all-gather.5
  89.9 25.5 all-gather.7
  117.6 92.2 all-gather.9
  212.0 90.4 all-gather.11
  304.4 91.2 all-gather.13
  412.1 32.5 reduce-scatter.1
